TPU v7x, 32 devices: a whole 2x2x4 slice. The times are simulated.
32 devices in a mesh: grp: 2 (over y), fs: 4 (over z), tp: 4 (over x, core).
Axes of the slice: x: 2, y: 2, z: 4, core: 2. Of those that a mesh axis runs over, the one named last changes fastest.
Arguments:
- tokens: bfloat16 [3072, 2048], P(('grp', 'fs'), 'tp'), parts along dimension 0, may hold values from -6 to 6
- mix_gain: float32 [2048], replicated, may hold values from 0.1 to 1.9
- w_signal: bfloat16 [2048, 1024], P('fs', 'tp'), may hold values from -0.125 to 0.125
- w_outer_gate: bfloat16 [2048, 1024], P('fs', 'tp'), may hold values from -0.125 to 0.125
- w_inner_gate: bfloat16 [2048, 1024], P('fs', 'tp'), may hold values from -0.125 to 0.125
- mix_taps: float32 [3, 1024], P(None, 'tp'), may hold values from -3 to 3
- w_mix_out: bfloat16 [1024, 2048], P('tp', 'fs'), may hold values from -0.1875 to 0.1875
- ffn_gain: float32 [2048], replicated, may hold values from 0.1 to 1.9
- w_gate: bfloat16 [2048, 5120], P('fs', 'tp'), may hold values from -0.125 to 0.125
- w_value: bfloat16 [2048, 5120], P('fs', 'tp'), may hold values from -0.125 to 0.125
- up_taps: float32 [2, 3, 5120], P(None, None, 'tp'), may hold values from -3 to 3
- up_bias: float32 [2, 5120], P(None, 'tp'), may hold values from -3 to 3
- w_down: bfloat16 [5120, 2048], P('tp', 'fs'), may hold values from -0.078125 to 0.078125
Outputs:
- layer_out: bfloat16 [3072, 2048], P(('grp', 'fs'), 'tp'), parts along dimension 0
There are 2 independent parts, one for each index of `grp`. A program takes and returns all parts, laid end to end along the dimension named above; an argument that names none is the same for every part. Nothing has to cross between parts.
All inputs are finite; a program needn't handle non-finite values.
Results may differ from a plain program's by a relative error of at most 0.022.
Values may be sent and summed in bfloat16 or wider, within the bound.
A program may use at most 64 MiB of HBM per device.

v0:
```python
import jax
import jax.numpy as jnp
from jax import lax
from jax.sharding import PartitionSpec as P

SEQS_DEV = 2


def conv_positions(values, taps):
    width = values.shape[1]
    blocks = values.reshape(SEQS_DEV, -1, width)
    length = blocks.shape[1]
    padded = jnp.pad(blocks, ((0, 0), (2, 0), (0, 0)))
    result = (
        padded[:, 0:length] * taps[0]
        + padded[:, 1 : length + 1] * taps[1]
        + padded[:, 2 : length + 2] * taps[2]
    )
    return result.reshape(-1, width)


def rms_norm(stream, gain):
    values = stream.astype(jnp.float32)
    scale = lax.rsqrt(jnp.mean(values * values, axis=-1, keepdims=True) + 1e-06)
    return (values * scale * gain).astype(jnp.bfloat16)


def on_device(
    tokens,
    mix_gain,
    w_signal,
    w_outer_gate,
    w_inner_gate,
    mix_taps,
    w_mix_out,
    ffn_gain,
    w_gate,
    w_value,
    up_taps,
    up_bias,
    w_down,
):
    whole = lax.all_gather(tokens, "tp", axis=1, tiled=True)
    normed = rms_norm(whole, mix_gain)
    pieces = (
        lax.all_gather(w_signal, "fs", axis=0, tiled=True),
        lax.all_gather(w_outer_gate, "fs", axis=0, tiled=True),
        lax.all_gather(w_inner_gate, "fs", axis=0, tiled=True),
    )
    columns = normed
    signal, outer, inner = tuple(
        (jnp.dot(columns, piece, preferred_element_type=jnp.float32) for piece in pieces)
    )
    signal = signal.astype(jnp.bfloat16).astype(jnp.float32)
    outer = outer.astype(jnp.bfloat16).astype(jnp.float32)
    inner = inner.astype(jnp.bfloat16).astype(jnp.float32)
    mixed = (outer * conv_positions(inner * signal, mix_taps)).astype(jnp.bfloat16)
    mix_terms = jnp.dot(
        mixed,
        lax.all_gather(w_mix_out, "fs", axis=1, tiled=True),
        preferred_element_type=jnp.float32,
    )
    mix_sum = lax.psum_scatter(
        mix_terms.astype(jnp.bfloat16), "tp", scatter_dimension=1, tiled=True
    ).astype(jnp.float32)
    resid = (tokens.astype(jnp.float32) + mix_sum).astype(jnp.bfloat16)
    whole_ffn = lax.all_gather(resid, "tp", axis=1, tiled=True)
    normed_ffn = rms_norm(whole_ffn, ffn_gain)
    pieces = (
        lax.all_gather(w_gate, "fs", axis=0, tiled=True),
        lax.all_gather(w_value, "fs", axis=0, tiled=True),
    )
    columns = normed_ffn
    gate = jnp.dot(columns, pieces[0], preferred_element_type=jnp.float32)
    value = jnp.dot(columns, pieces[1], preferred_element_type=jnp.float32)
    gate = gate.astype(jnp.bfloat16).astype(jnp.float32)
    value = value.astype(jnp.bfloat16).astype(jnp.float32)
    gate_conv = conv_positions(gate, up_taps[0]) + up_bias[0]
    value_conv = conv_positions(value, up_taps[1]) + up_bias[1]
    hidden = (jax.nn.silu(gate_conv) * value_conv).astype(jnp.bfloat16)
    ffn_terms = jnp.dot(
        hidden, lax.all_gather(w_down, "fs", axis=1, tiled=True), preferred_element_type=jnp.float32
    )
    ffn_sum = lax.psum_scatter(
        ffn_terms.astype(jnp.bfloat16), "tp", scatter_dimension=1, tiled=True
    ).astype(jnp.float32)
    return (resid.astype(jnp.float32) + ffn_sum).astype(jnp.bfloat16)


def solution(mesh):
    placed = (
        P(("grp", "fs"), "tp"),
        P(),
        P("fs", "tp"),
        P("fs", "tp"),
        P("fs", "tp"),
        P(None, "tp"),
        P("tp", "fs"),
        P(),
        P("fs", "tp"),
        P("fs", "tp"),
        P(None, None, "tp"),
        P(None, "tp"),
        P("tp", "fs"),
    )
    return jax.shard_map(
        on_device, mesh=mesh, in_specs=placed, out_specs=P(("grp", "fs"), "tp"), check_vma=False
    )
```

profile of v0, /device:TPU:0, one launch (start us, length us, event | category | flops | bytes accessed | tf_op | source)
XLA Modules:
  0.0 537.4 jit_solution(5827497235861300328)
XLA Ops:
  6.5 0.7 all-gather.10.cloned.1.call-update
  10.0 0.8 fusion.32
  10.8 20.5 %all-gather.10.cloned.1.call-done = bf16[384,2048]{1,0:T(8,128)(2,1)} async-done(((bf16[384,512]{1,0:T(8,128)(2,1)}), bf16[384,2048]{1,0:T(8,128)(2,1)}) %all-gather.10.cloned.1.call-update) | async-done | bytes 1572880 | tf_op jit(solution)/shard_map/all_gather | solution.py:43
  31.3 1.8 fusion
  33.1 27.8 %all-gather.14.cloned.1.call-done = bf16[2048,256]{1,0:T(8,128)(2,1)} async-done(((bf16[512,256]{1,0:T(8,128)(2,1)}), bf16[2048,256]{1,0:T(8,128)(2,1)}) %all-gather.14.cloned.1.call-update) | async-done | bytes 1048592 | tf_op jit(solution)/shard_map/all_gather | solution.py:48
  60.9 2.3 fusion.18
  63.2 26.6 %all-gather.16.cloned.1.call-done = bf16[2048,256]{1,0:T(8,128)(2,1)} async-done(((bf16[512,256]{1,0:T(8,128)(2,1)}), bf16[2048,256]{1,0:T(8,128)(2,1)}) %all-gather.16.cloned.1.call-update) | async-done | bytes 1048592 | tf_op jit(solution)/shard_map/all_gather | solution.py:46
  89.8 1.8 fusion.17
  91.8 26.8 %all-gather.12.cloned.1.call-done = bf16[2048,256]{1,0:T(8,128)(2,1)} async-done(((bf16[512,256]{1,0:T(8,128)(2,1)}), bf16[2048,256]{1,0:T(8,128)(2,1)}) %all-gather.12.cloned.1.call-update) | async-done | bytes 1048592 | tf_op jit(solution)/shard_map/all_gather | solution.py:47
  118.6 28.8 %all-gather.18.cloned.1.call-done = bf16[256,2048]{1,0:T(8,128)(2,1)} async-done(((bf16[256,512]{1,0:T(8,128)(2,1)}), bf16[256,2048]{1,0:T(8,128)(2,1)}) %all-gather.18.cloned.1.call-update) | async-done | bytes 1048592 | tf_op jit(solution)/shard_map/all_gather | solution.py:60
  147.5 4.6 convolution_convert_fusion.3
  152.1 27.5 %reduce-scatter.3.cloned.1.call-done = bf16[384,512]{1,0:T(8,128)(2,1)} async-done(((bf16[384,2048]{1,0:T(8,128)(2,1)}), bf16[384,512]{1,0:T(8,128)(2,1)}) %reduce-scatter.3.cloned.1.call-update) | async-done | bytes 393232 | tf_op jit(solution)/shard_map/reduce_scatter | solution.py:63
  179.6 1.8 add_convert_fusion.1
  184.4 16.9 %all-gather.20.cloned.1.call-done = bf16[384,2048]{1,0:T(8,128)(2,1)} async-done(((bf16[384,512]{1,0:T(8,128)(2,1)}), bf16[384,2048]{1,0:T(8,128)(2,1)}) %all-gather.20.cloned.1.call-update) | async-done | bytes 1572880 | tf_op jit(solution)/shard_map/all_gather | solution.py:67
  201.3 1.8 fusion.3
  203.1 97.8 %all-gather.24.cloned.1.call-done = bf16[2048,1280]{1,0:T(8,128)(2,1)} async-done(((bf16[512,1280]{1,0:T(8,128)(2,1)}), bf16[2048,1280]{1,0:T(8,128)(2,1)}) %all-gather.24.cloned.1.call-update) | async-done | bytes 5242896 | tf_op jit(solution)/shard_map/all_gather | solution.py:71
  300.9 5.2 convolution_convert_fusion.1
  306.3 92.6 %all-gather.22.cloned.1.call-done = bf16[2048,1280]{1,0:T(8,128)(2,1)} async-done(((bf16[512,1280]{1,0:T(8,128)(2,1)}), bf16[2048,1280]{1,0:T(8,128)(2,1)}) %all-gather.22.cloned.1.call-update) | async-done | bytes 5242896 | tf_op jit(solution)/shard_map/all_gather | solution.py:70
  398.9 4.8 convolution_convert_fusion.2
  404.4 1.2 fusion.8
  406.2 90.5 %all-gather.26.cloned.1.call-done = bf16[1280,2048]{1,0:T(8,128)(2,1)} async-done(((bf16[1280,512]{1,0:T(8,128)(2,1)}), bf16[1280,2048]{1,0:T(8,128)(2,1)}) %all-gather.26.cloned.1.call-update) | async-done | bytes 5242896 | tf_op jit(solution)/shard_map/all_gather | solution.py:82
  496.7 5.9 %convolution_convert_fusion = bf16[384,2048]{1,0:T(8,128)(2,1)} fusion(bf16[384,1280]{1,0:T(8,128)(2,1)S(1)} %fusion.15, bf16[1280,2048]{1,0:T(8,128)(2,1)} %all-gather.26.cloned.1.call-done), kind=kOutput, calls=%fused_computation.10 | convolution fusion | flops 2014052352 | bytes 7798784 | tf_op jit(solution)/shard_map/dot_general | solution.py:81
  502.6 26.5 %reduce-scatter.5.cloned.1.call-done = bf16[384,512]{1,0:T(8,128)(2,1)} async-done(((bf16[384,2048]{1,0:T(8,128)(2,1)}), bf16[384,512]{1,0:T(8,128)(2,1)}) %reduce-scatter.5.cloned.1.call-update) | async-done | bytes 393232 | tf_op jit(solution)/shard_map/reduce_scatter | solution.py:84
  529.1 1.8 add_convert_fusion
  (59 shorter events, 7.1 us)
Async XLA Ops:
  6.5 54.3 %copy-start.13 = (f32[2048]{0:T(1024)S(1)}, f32[2048]{0:T(1024)}, u32[]{:S(2)}) copy-start(f32[2048]{0:T(1024)} %param.14) | copy-start | bytes 24580
  6.5 24.7 %all-gather.10.cloned.1.call-start = ((), (), s32[]{:S(2)}) async-start(), calls=%async_computation.2 | async-start | bytes 1966080 | tf_op jit(solution)/shard_map/all_gather | solution.py:43
  7.3 53.6 %all-gather.14.cloned.1.call-start = ((), (), s32[]{:S(2)}) async-start(), calls=%async_computation.4 | async-start | bytes 1310720 | tf_op jit(solution)/shard_map/all_gather | solution.py:48
  8.0 81.8 %all-gather.16.cloned.1.call-start = ((), (), s32[]{:S(2)}) async-start(), calls=%async_computation.5 | async-start | bytes 1310720 | tf_op jit(solution)/shard_map/all_gather | solution.py:46
  8.7 109.9 %all-gather.12.cloned.1.call-start = ((), (), s32[]{:S(2)}) async-start(), calls=%async_computation.3 | async-start | bytes 1310720 | tf_op jit(solution)/shard_map/all_gather | solution.py:47
  9.3 138.1 %all-gather.18.cloned.1.call-start = ((), (), s32[]{:S(2)}) async-start(), calls=%async_computation.6 | async-start | bytes 1310720 | tf_op jit(solution)/shard_map/all_gather | solution.py:60
  9.9 169.7 %reduce-scatter.3.cloned.1.call-start = ((), (), s32[]{:S(2)}) async-start(), calls=%async_computation.7 | async-start | bytes 1966080 | tf_op jit(solution)/shard_map/reduce_scatter | solution.py:63
  33.1 56.8 %copy-start.1 = (bf16[384,2048]{1,0:T(8,128)(2,1)S(1)}, bf16[384,2048]{1,0:T(8,128)(2,1)}, u32[]{:S(2)}) copy-start(bf16[384,2048]{1,0:T(8,128)(2,1)} %all-gather.10.cloned.1.call-done) | copy-start | bytes 4718596
  147.5 32.2 %copy-start.3 = (bf16[384,512]{1,0:T(8,128)(2,1)S(1)}, bf16[384,512]{1,0:T(8,128)(2,1)}, u32[]{:S(2)}) copy-start(bf16[384,512]{1,0:T(8,128)(2,1)} %param.13) | copy-start | bytes 1179652
  152.1 49.2 %all-gather.20.cloned.1.call-start = ((), (), s32[]{:S(2)}) async-start(), calls=%async_computation.8 | async-start | bytes 1966080 | tf_op jit(solution)/shard_map/all_gather | solution.py:67
  181.5 2.2 copy-start.11
  181.5 2.2 copy-start.10
  181.5 119.4 %all-gather.24.cloned.1.call-start = ((), (), s32[]{:S(2)}) async-start(), calls=%async_computation.10 | async-start | bytes 6553600 | tf_op jit(solution)/shard_map/all_gather | solution.py:71
  182.3 118.7 %copy-start.14 = (f32[2048]{0:T(1024)S(1)}, f32[2048]{0:T(1024)}, u32[]{:S(2)}) copy-start(f32[2048]{0:T(1024)} %param.20) | copy-start | bytes 24580
  182.3 216.6 %all-gather.22.cloned.1.call-start = ((), (), s32[]{:S(2)}) async-start(), calls=%async_computation.9 | async-start | bytes 6553600 | tf_op jit(solution)/shard_map/all_gather | solution.py:70
  183.0 313.7 %all-gather.26.cloned.1.call-start = ((), (), s32[]{:S(2)}) async-start(), calls=%async_computation.11 | async-start | bytes 6553600 | tf_op jit(solution)/shard_map/all_gather | solution.py:82
  183.6 345.5 %reduce-scatter.5.cloned.1.call-start = ((), (), s32[]{:S(2)}) async-start(), calls=%async_computation.12 | async-start | bytes 1966080 | tf_op jit(solution)/shard_map/reduce_scatter | solution.py:84
  203.1 103.1 %copy-start.12 = (f32[384]{0:T(512)}, f32[384]{0:T(512)S(1)}, u32[]{:S(2)}) copy-start(f32[384]{0:T(512)S(1)} %add_rsqrt_fusion) | copy-start | bytes 4612
  306.1 92.8 %copy-start.2 = (bf16[384,2048]{1,0:T(8,128)(2,1)S(1)}, bf16[384,2048]{1,0:T(8,128)(2,1)}, u32[]{:S(2)}) copy-start(bf16[384,2048]{1,0:T(8,128)(2,1)} %all-gather.20.cloned.1.call-done) | copy-start | bytes 4718596
  403.7 0.7 copy-start.6
  403.7 0.7 copy-start.7
  403.7 0.7 copy-start.8
  403.7 0.7 copy-start.9
  406.2 122.9 %copy-start = (bf16[384,512]{1,0:T(8,128)(2,1)S(1)}, bf16[384,512]{1,0:T(8,128)(2,1)}, u32[]{:S(2)}) copy-start(bf16[384,512]{1,0:T(8,128)(2,1)} %add_convert_fusion.1) | copy-start | bytes 1179652
  (2 other events, 1.4 us)
Sparse Core Ops, SparseCore 0:
  8.9 22.3 all-gather.9
  32.8 27.9 all-gather.13
  62.4 27.3 all-gather.15
  91.3 27.3 all-gather.11
  120.1 27.3 all-gather.17
  152.2 27.3 reduce-scatter.2
  181.6 19.6 all-gather.19
  202.8 98.0 all-gather.23
  302.5 96.3 all-gather.21
  400.3 96.3 all-gather.25
  502.7 26.3 reduce-scatter.4
where the time goes:
time: 538 us; the launch traced here: 537 us
  waiting for transfers between devices  488 us (91%)
  matrix products  24.6 us (5%)
  between operations  13.4 us (2%)
  other arithmetic  9.39 us (2%)
    all_gather x1, waiting for transfers between devices, on_device(): lax.all_gather(w_value, 'fs', axis=0, tiled=True)  97.8 us
    all_gather x1, waiting for transfers between devices, on_device(): lax.all_gather(w_gate, 'fs', axis=0, tiled=True)  92.6 us
    all_gather x1, waiting for transfers between devices, on_device(): lax.all_gather(w_down, 'fs', axis=1, tiled=True)  90.5 us
    all_gather x1, waiting for transfers between devices, on_device(): lax.all_gather(w_mix_out, 'fs', axis=1, tiled=True)  28.8 us
    all_gather x1, waiting for transfers between devices, on_device(): lax.all_gather(w_inner_gate, 'fs', axis=0, tiled=True)  27.8 us
    reduce_scatter x1, waiting for transfers between devices, on_device(): lax.psum_scatter(mix_terms.astype(jnp.bfloat16), 'tp', scatter_dimension=...  27.5 us
    all_gather x1, waiting for transfers between devices, on_device(): lax.all_gather(w_outer_gate, 'fs', axis=0, tiled=True)  26.8 us
    all_gather x1, waiting for transfers between devices, on_device(): lax.all_gather(w_signal, 'fs', axis=0, tiled=True)  26.6 us
  transfers between devices with their start and end apart: 11, of which 11 were waited for; matrix products, arithmetic and copies ran while one was open for 4% of the time, Pallas kernels for 0%

commit v1 on v0

--- a/solution.py
+++ b/solution.py
@@ -4,6 +4,11 @@
 from jax.sharding import PartitionSpec as P
 
 SEQS_DEV = 2
+
+
+def all_by_exchange(x, mesh_axis, d):
+    stack = jnp.stack([x] * lax.axis_size(mesh_axis))
+    return jnp.concatenate(lax.all_to_all(stack, mesh_axis, 0, 0), axis=d)
 
 
 def conv_positions(values, taps):
@@ -45,7 +50,7 @@
     pieces = (
         lax.all_gather(w_signal, "fs", axis=0, tiled=True),
         lax.all_gather(w_outer_gate, "fs", axis=0, tiled=True),
-        lax.all_gather(w_inner_gate, "fs", axis=0, tiled=True),
+        all_by_exchange(w_inner_gate, "fs", 0),
     )
     columns = normed
     signal, outer, inner = tuple(

time: 538 us -> 510 us (0.948)
  waiting for transfers between devices: 488 us -> 451 us
  starting transfers between devices: 0.39 us -> 6.79 us
    all_gather x1 -> x0, waiting for transfers between devices: 27.8 us -> none  [on_device(): lax.all_gather(w_inner_gate, 'fs', axis=0, tiled=True)]
    all_gather x1, waiting for transfers between devices: 26.6 us -> 15.7 us  [on_device(): lax.all_gather(w_signal, 'fs', axis=0, tiled=True)]
    all_to_all x0 -> x1, waiting for transfers between devices: none -> 9.89 us  [all_by_exchange(): return jnp.concatenate(lax.all_to_all(stack, mesh_axis, 0, 0), axis=d)]
    all_gather x1, waiting for transfers between devices: 20.5 us -> 13.4 us  [on_device(): whole = lax.all_gather(tokens, 'tp', axis=1, tiled=True)]
    all_to_all x0 -> x1, starting transfers between devices: none -> 6.48 us  [all_by_exchange(): return jnp.concatenate(lax.all_to_all(stack, mesh_axis, 0, 0), axis=d)]
where the time goes in v1:
time: 510 us; the launch traced here: 509 us
  waiting for transfers between devices  451 us (88%)
  matrix products  24.4 us (5%)
  between operations  13.7 us (3%)
  other arithmetic  9.38 us (2%)
  starting transfers between devices  6.79 us (1%)
    all_gather x1, waiting for transfers between devices, on_device(): lax.all_gather(w_value, 'fs', axis=0, tiled=True)  97.8 us
    all_gather x1, waiting for transfers between devices, on_device(): lax.all_gather(w_gate, 'fs', axis=0, tiled=True)  92.6 us
    all_gather x1, waiting for transfers between devices, on_device(): lax.all_gather(w_down, 'fs', axis=1, tiled=True)  90.7 us
    all_gather x1, waiting for transfers between devices, on_device(): lax.all_gather(w_mix_out, 'fs', axis=1, tiled=True)  28.8 us
    reduce_scatter x1, waiting for transfers between devices, on_device(): lax.psum_scatter(mix_terms.astype(jnp.bfloat16), 'tp', scatter_dimension=...  27.5 us
    all_gather x1, waiting for transfers between devices, on_device(): lax.all_gather(w_outer_gate, 'fs', axis=0, tiled=True)  27 us
    reduce_scatter x1, waiting for transfers between devices, on_device(): lax.psum_scatter(ffn_terms.astype(jnp.bfloat16), 'tp', scatter_dimension=...  26.5 us
    all_gather x1, waiting for transfers between devices, on_device(): whole_ffn = lax.all_gather(resid, 'tp', axis=1, tiled=True)  16.7 us
  transfers between devices with their start and end apart: 11, of which 11 were waited for; matrix products, arithmetic and copies ran while one was open for 4% of the time, Pallas kernels for 0%

profile of v1, /device:TPU:0, one launch (start us, length us, event | category | flops | bytes accessed | tf_op | source)
XLA Modules:
  0.0 509.1 jit_solution(11357916685845319055)
XLA Ops:
  8.8 2.0 stack.2
  10.8 6.5 %all-to-all-start = ((bf16[4,512,256]{2,1,0:T(8,128)(2,1)}), bf16[4,512,256]{2,1,0:T(8,128)(2,1)S(1)}, u32[]{:S(2)}, u32[]{:S(2)}) async-start(bf16[4,512,256]{2,1,0:T(8,128)(2,1)} %stack.2), calls=%async_computation | async-start | bytes 2097152 | tf_op jit(solution)/shard_map/all_to_all | solution.py:11
  17.9 13.4 %all-gather.9.cloned.1.call-done = bf16[384,2048]{1,0:T(8,128)(2,1)} async-done(((bf16[384,512]{1,0:T(8,128)(2,1)}), bf16[384,2048]{1,0:T(8,128)(2,1)}) %all-gather.9.cloned.1.call-update) | async-done | bytes 1572880 | tf_op jit(solution)/shard_map/all_gather | solution.py:48
  31.3 1.8 fusion
  33.1 9.9 %all-to-all-done = bf16[4,512,256]{2,1,0:T(8,128)(2,1)S(1)} async-done(((bf16[4,512,256]{2,1,0:T(8,128)(2,1)}), bf16[4,512,256]{2,1,0:T(8,128)(2,1)S(1)}, u32[]{:S(2)}, u32[]{:S(2)}) %all-to-all-start) | async-done | bytes 1048608 | tf_op jit(solution)/shard_map/all_to_all | solution.py:11
  43.0 2.1 fusion.18
  45.1 15.7 %all-gather.13.cloned.1.call-done = bf16[2048,256]{1,0:T(8,128)(2,1)} async-done(((bf16[512,256]{1,0:T(8,128)(2,1)}), bf16[2048,256]{1,0:T(8,128)(2,1)}) %all-gather.13.cloned.1.call-update) | async-done | bytes 1048592 | tf_op jit(solution)/shard_map/all_gather | solution.py:51
  60.9 1.8 fusion.17
  62.8 27.0 %all-gather.11.cloned.1.call-done = bf16[2048,256]{1,0:T(8,128)(2,1)} async-done(((bf16[512,256]{1,0:T(8,128)(2,1)}), bf16[2048,256]{1,0:T(8,128)(2,1)}) %all-gather.11.cloned.1.call-update) | async-done | bytes 1048592 | tf_op jit(solution)/shard_map/all_gather | solution.py:52
  89.8 28.8 %all-gather.15.cloned.1.call-done = bf16[256,2048]{1,0:T(8,128)(2,1)} async-done(((bf16[256,512]{1,0:T(8,128)(2,1)}), bf16[256,2048]{1,0:T(8,128)(2,1)}) %all-gather.15.cloned.1.call-update) | async-done | bytes 1048592 | tf_op jit(solution)/shard_map/all_gather | solution.py:65
  118.7 4.6 convolution_convert_fusion.3
  123.3 27.5 %reduce-scatter.3.cloned.1.call-done = bf16[384,512]{1,0:T(8,128)(2,1)} async-done(((bf16[384,2048]{1,0:T(8,128)(2,1)}), bf16[384,512]{1,0:T(8,128)(2,1)}) %reduce-scatter.3.cloned.1.call-update) | async-done | bytes 393232 | tf_op jit(solution)/shard_map/reduce_scatter | solution.py:68
  150.8 1.8 add_convert_fusion.1
  155.7 16.7 %all-gather.17.cloned.1.call-done = bf16[384,2048]{1,0:T(8,128)(2,1)} async-done(((bf16[384,512]{1,0:T(8,128)(2,1)}), bf16[384,2048]{1,0:T(8,128)(2,1)}) %all-gather.17.cloned.1.call-update) | async-done | bytes 1572880 | tf_op jit(solution)/shard_map/all_gather | solution.py:72
  172.5 1.8 fusion.3
  174.3 97.8 %all-gather.21.cloned.1.call-done = bf16[2048,1280]{1,0:T(8,128)(2,1)} async-done(((bf16[512,1280]{1,0:T(8,128)(2,1)}), bf16[2048,1280]{1,0:T(8,128)(2,1)}) %all-gather.21.cloned.1.call-update) | async-done | bytes 5242896 | tf_op jit(solution)/shard_map/all_gather | solution.py:76
  272.1 5.2 %convolution_convert_fusion.1 = bf16[384,1280]{1,0:T(8,128)(2,1)S(1)} fusion(bf16[2048,1280]{1,0:T(8,128)(2,1)} %all-gather.21.cloned.1.call-done, bf16[384,2048]{1,0:T(8,128)(2,1)} %all-gather.17.cloned.1.call-done, f32[2048]{0:T(1024)S(1)} %copy-done.15, f32[384]{0:T(512)S(1)} %add_rsqrt_fusion), kind=kOutput, calls=%fused_computation.11 | convolution fusion | flops 2016903168 | bytes 7808512 | tf_op jit(solution)/shard_map/dot_general | solution.py:80
  277.5 92.6 %all-gather.19.cloned.1.call-done = bf16[2048,1280]{1,0:T(8,128)(2,1)} async-done(((bf16[512,1280]{1,0:T(8,128)(2,1)}), bf16[2048,1280]{1,0:T(8,128)(2,1)}) %all-gather.19.cloned.1.call-update) | async-done | bytes 5242896 | tf_op jit(solution)/shard_map/all_gather | solution.py:75
  370.1 4.8 convolution_convert_fusion.2
  375.6 1.2 fusion.8
  377.4 90.7 %all-gather.23.cloned.1.call-done = bf16[1280,2048]{1,0:T(8,128)(2,1)} async-done(((bf16[1280,512]{1,0:T(8,128)(2,1)}), bf16[1280,2048]{1,0:T(8,128)(2,1)}) %all-gather.23.cloned.1.call-update) | async-done | bytes 5242896 | tf_op jit(solution)/shard_map/all_gather | solution.py:87
  468.1 5.9 %convolution_convert_fusion = bf16[384,2048]{1,0:T(8,128)(2,1)} fusion(bf16[384,1280]{1,0:T(8,128)(2,1)S(1)} %fusion.15, bf16[1280,2048]{1,0:T(8,128)(2,1)} %all-gather.23.cloned.1.call-done), kind=kOutput, calls=%fused_computation.10 | convolution fusion | flops 2014052352 | bytes 7798784 | tf_op jit(solution)/shard_map/dot_general | solution.py:86
  473.9 26.5 %reduce-scatter.5.cloned.1.call-done = bf16[384,512]{1,0:T(8,128)(2,1)} async-done(((bf16[384,2048]{1,0:T(8,128)(2,1)}), bf16[384,512]{1,0:T(8,128)(2,1)}) %reduce-scatter.5.cloned.1.call-update) | async-done | bytes 393232 | tf_op jit(solution)/shard_map/reduce_scatter | solution.py:89
  500.4 1.8 add_convert_fusion
  (61 shorter events, 7.4 us)
Async XLA Ops:
  6.5 24.7 %all-gather.9.cloned.1.call-start = ((), (), s32[]{:S(2)}) async-start(), calls=%async_computation.3 | async-start | bytes 1966080 | tf_op jit(solution)/shard_map/all_gather | solution.py:48
  7.3 53.6 %all-gather.13.cloned.1.call-start = ((), (), s32[]{:S(2)}) async-start(), calls=%async_computation.5 | async-start | bytes 1310720 | tf_op jit(solution)/shard_map/all_gather | solution.py:51
  8.0 9.8 %copy-start.12 = (f32[3,256]{1,0:T(4,128)S(1)}, f32[3,256]{1,0:T(4,128)}, u32[]{:S(2)}) copy-start(f32[3,256]{1,0:T(4,128)} %param.18) | copy-start | bytes 9220
  8.0 81.8 %all-gather.11.cloned.1.call-start = ((), (), s32[]{:S(2)}) async-start(), calls=%async_computation.4 | async-start | bytes 1310720 | tf_op jit(solution)/shard_map/all_gather | solution.py:52
  10.8 32.2 %copy-start.14 = (f32[2048]{0:T(1024)S(1)}, f32[2048]{0:T(1024)}, u32[]{:S(2)}) copy-start(f32[2048]{0:T(1024)} %param.14) | copy-start | bytes 24580
  10.8 32.2 %all-to-all-start = ((bf16[4,512,256]{2,1,0:T(8,128)(2,1)}), bf16[4,512,256]{2,1,0:T(8,128)(2,1)S(1)}, u32[]{:S(2)}, u32[]{:S(2)}) async-start(bf16[4,512,256]{2,1,0:T(8,128)(2,1)} %stack.2), calls=%async_computation | async-start | bytes 2097152 | tf_op jit(solution)/shard_map/all_to_all | solution.py:11
  17.2 101.4 %all-gather.15.cloned.1.call-start = ((), (), s32[]{:S(2)}) async-start(), calls=%async_computation.6 | async-start | bytes 1310720 | tf_op jit(solution)/shard_map/all_gather | solution.py:65
  17.8 133.0 %reduce-scatter.3.cloned.1.call-start = ((), (), s32[]{:S(2)}) async-start(), calls=%async_computation.7 | async-start | bytes 1966080 | tf_op jit(solution)/shard_map/reduce_scatter | solution.py:68
  43.0 17.9 %copy-start.1 = (bf16[384,2048]{1,0:T(8,128)(2,1)S(1)}, bf16[384,2048]{1,0:T(8,128)(2,1)}, u32[]{:S(2)}) copy-start(bf16[384,2048]{1,0:T(8,128)(2,1)} %all-gather.9.cloned.1.call-done) | copy-start | bytes 4718596
  118.6 32.2 %copy-start.3 = (bf16[384,512]{1,0:T(8,128)(2,1)S(1)}, bf16[384,512]{1,0:T(8,128)(2,1)}, u32[]{:S(2)}) copy-start(bf16[384,512]{1,0:T(8,128)(2,1)} %param.13) | copy-start | bytes 1179652
  123.3 49.2 %all-gather.17.cloned.1.call-start = ((), (), s32[]{:S(2)}) async-start(), calls=%async_computation.8 | async-start | bytes 1966080 | tf_op jit(solution)/shard_map/all_gather | solution.py:72
  152.7 2.3 copy-start.11
  152.7 2.4 copy-start.10
  152.7 119.4 %all-gather.21.cloned.1.call-start = ((), (), s32[]{:S(2)}) async-start(), calls=%async_computation.10 | async-start | bytes 6553600 | tf_op jit(solution)/shard_map/all_gather | solution.py:76
  153.5 118.7 %copy-start.15 = (f32[2048]{0:T(1024)S(1)}, f32[2048]{0:T(1024)}, u32[]{:S(2)}) copy-start(f32[2048]{0:T(1024)} %param.20) | copy-start | bytes 24580
  153.5 216.6 %all-gather.19.cloned.1.call-start = ((), (), s32[]{:S(2)}) async-start(), calls=%async_computation.9 | async-start | bytes 6553600 | tf_op jit(solution)/shard_map/all_gather | solution.py:75
  154.2 313.8 %all-gather.23.cloned.1.call-start = ((), (), s32[]{:S(2)}) async-start(), calls=%async_computation.11 | async-start | bytes 6553600 | tf_op jit(solution)/shard_map/all_gather | solution.py:87
  155.0 345.5 %reduce-scatter.5.cloned.1.call-start = ((), (), s32[]{:S(2)}) async-start(), calls=%async_computation.12 | async-start | bytes 1966080 | tf_op jit(solution)/shard_map/reduce_scatter | solution.py:89
  174.3 103.1 %copy-start.13 = (f32[384]{0:T(512)}, f32[384]{0:T(512)S(1)}, u32[]{:S(2)}) copy-start(f32[384]{0:T(512)S(1)} %add_rsqrt_fusion) | copy-start | bytes 4612
  277.4 92.7 %copy-start.2 = (bf16[384,2048]{1,0:T(8,128)(2,1)S(1)}, bf16[384,2048]{1,0:T(8,128)(2,1)}, u32[]{:S(2)}) copy-start(bf16[384,2048]{1,0:T(8,128)(2,1)} %all-gather.17.cloned.1.call-done) | copy-start | bytes 4718596
  374.9 0.7 copy-start.7
  374.9 0.7 copy-start.8
  374.9 0.7 copy-start.9
  377.4 123.1 %copy-start = (bf16[384,512]{1,0:T(8,128)(2,1)S(1)}, bf16[384,512]{1,0:T(8,128)(2,1)}, u32[]{:S(2)}) copy-start(bf16[384,512]{1,0:T(8,128)(2,1)} %add_convert_fusion.1) | copy-start | bytes 1179652
  (3 other events, 2.1 us)
Sparse Core Ops, SparseCore 0:
  8.9 22.3 all-gather.8
  32.8 27.9 all-gather.12
  62.4 27.3 all-gather.10
  91.3 27.3 all-gather.14
  123.4 27.3 reduce-scatter.2
  152.8 19.6 all-gather.16
  174.0 98.0 all-gather.20
  273.7 96.3 all-gather.18
  371.7 96.3 all-gather.22
  474.1 26.3 reduce-scatter.4
